TPU v7x, 32 devices: a whole 2x2x4 slice. The times are simulated.
32 devices in a mesh: rep: 2 (over x), fs: 8 (over z, y), tp: 2 (over core).
Axes of the slice: x: 2, y: 2, z: 4, core: 2. Of those that a mesh axis runs over, the one named last changes fastest.
Arguments:
- stream: bfloat16 [16, 1024, 2048], P(('rep', 'fs'), None, 'tp'), may hold values from -6 to 6
- norm_gain: float32 [2048], replicated, may hold values from 0.1 to 1.9
- w_in: float32 [2048, 512], P('fs', 'tp'), may hold values from -0.125 to 0.125
- s_in: float32 [512], P(('tp', 'fs')), may hold values from 0.1 to 1.9
- pool_w: bfloat16 [4, 128, 128], replicated, may hold values from -0.5 to 0.5
- w_out: float32 [512, 2048], P('fs', 'tp'), may hold values from -0.25 to 0.25
- s_out: float32 [2048], P(('tp', 'fs')), may hold values from 0.1 to 1.9
- ffn_gain: float32 [2048], replicated, may hold values from 0.1 to 1.9
- w_up: float32 [2048, 8192], P('fs', 'tp'), may hold values from -0.125 to 0.125
- s_up: float32 [8192], P(('tp', 'fs')), may hold values from 0.1 to 1.9
- w_down: float32 [8192, 2048], P('tp', 'fs'), may hold values from -0.0625 to 0.0625
- s_down: float32 [2048], P('fs'), may hold values from 0.1 to 1.9
Outputs:
- result: bfloat16 [16, 1024, 2048], P(('rep', 'fs'), None, 'tp')
All inputs are finite; a program needn't handle non-finite values.
Results may differ from a plain program's by a relative error of at most 0.012.
Values may be sent and summed in bfloat16 or wider, within the bound.
A program may use at most 128 MiB of HBM per device.

v0:
```python
import functools

import jax
import jax.numpy as jnp
from jax import lax
from jax.experimental import pallas as pl
from jax.experimental.pallas import tpu as pltpu
from jax.sharding import PartitionSpec as P

GROUP = 128


epsilon = 0.25
bf16 = jnp.bfloat16
f32 = jnp.float32


def dot(left, right):
    return jnp.dot(left, right, preferred_element_type=f32)


def rms_rows(values, gain):
    floats = values.astype(f32)
    scale = lax.rsqrt(jnp.mean(floats * floats, axis=-1, keepdims=True) + epsilon)
    return (floats * scale * gain).astype(bf16)


def shifted(value, axis_name, count, offset):
    return lax.ppermute(value, axis_name, [(i, (i + offset) % count) for i in range(count)])


def swap_gather(value, axis_name, count, axis):
    index = lax.axis_index(axis_name)
    width = value.shape[axis]
    shape = list(value.shape)
    shape[axis] = width * count
    if count == 2:
        other = shifted(value, axis_name, count, 1)
        low = jnp.where(index == 0, value, other)
        high = jnp.where(index == 0, other, value)
        return jnp.concatenate([low, high], axis=axis)
    full = jnp.zeros(shape, value.dtype)
    full = lax.dynamic_update_slice_in_dim(full, value, index * width, axis)
    for offset in range(1, count):
        piece = shifted(value, axis_name, count, offset)
        origin = (index - offset) % count
        full = lax.dynamic_update_slice_in_dim(full, piece, origin * width, axis)
    return full


def fs_sent(value, factors, offset_a, offset_b):
    n_a, n_b = factors
    pairs = []
    for i in range(n_a * n_b):
        pairs.append((i, ((i // n_b) ^ offset_a) * n_b + ((i % n_b) ^ offset_b)))
    return lax.ppermute(value, "fs", pairs)


def fs_pieces(value, factors):
    n_a, n_b = factors
    rows = [[value] for _ in range(n_a)]
    for x in range(1, n_a):
        rows[x] = [fs_sent(value, factors, x, 0)]
    for y in range(1, n_b):
        for x in range(n_a):
            rows[x].append(fs_sent(rows[x][0], factors, 0, y))
    return rows


def fs_origin(factors, x, y):
    index = lax.axis_index("fs")
    return ((index // factors[1]) ^ x) * factors[1] + ((index % factors[1]) ^ y)


def placed(rows, factors):
    block = rows[0][0].shape[0]
    width = rows[0][0].shape[1]
    full = jnp.zeros((block * factors[0] * factors[1], width), rows[0][0].dtype)
    for y in range(factors[1]):
        for x in range(factors[0]):
            full = lax.dynamic_update_slice_in_dim(
                full, rows[x][y], fs_origin(factors, x, y) * block, 0
            )
    return full


def pool_local(pool_in, first):
    length, width = pool_in.shape
    positions = jnp.arange(length, dtype=jnp.int32)
    source = positions[None, :]
    target = positions[:, None]
    group_of = (first + jnp.arange(width, dtype=jnp.int32)) // GROUP
    means = jnp.zeros((length, width), f32)
    for level in range(4):
        half = 2**level
        band_ones = ((source >= target - half) & (source < target + half)).astype(bf16)
        counts = (jnp.minimum(positions + half, length) - jnp.maximum(positions - half, 0)).astype(f32)
        sums = dot(band_ones, pool_in) / counts[:, None]
        means = jnp.where(group_of[None, :] == level, sums, means)
    return (means - pool_in.astype(f32)).astype(bf16)


def on_device(
    n_rep, n_fs, n_tp,
    stream, norm_gain, w_in, s_in, pool_w, w_out, s_out, ffn_gain, w_up, s_up, w_down, s_down,
):
    rep = lax.axis_index("rep")
    tokens = stream[0]
    length, local_width = tokens.shape
    hidden_width = w_up.shape[1] // n_rep

    n_a = n_tp * max(1, 4 // n_tp)
    factors = (n_a, n_fs // n_a)

    scales = jnp.concatenate([s_in, s_out, s_up, s_down])[None]
    scale_rows = [
        [scales if x == y == 0 else fs_sent(scales, factors, x, y) for y in range(factors[1])]
        for x in range(n_a)
    ]
    scales = placed(scale_rows, factors)
    ends, at = [], 0
    for part in (s_in, s_out, s_up, s_down):
        ends.append(scales[:, at:at + part.shape[0]])
        at += part.shape[0]
    scale_in, scale_out, scale_up = (part.reshape(-1) for part in ends[:3])
    scale_down = ends[3]

    in_rows = fs_pieces(w_in.astype(bf16), factors)
    out_rows = fs_pieces(w_out.astype(bf16), factors)
    w_in_all = placed(in_rows, factors)
    w_out_all = placed(out_rows, factors)

    up_own = lax.dynamic_slice_in_dim(w_up, rep * hidden_width, hidden_width, 1).astype(bf16)
    up_rows = fs_pieces(up_own, factors)
    up_all = placed(up_rows, factors)
    down_own = lax.dynamic_slice_in_dim(w_down, rep * hidden_width, hidden_width, 0).astype(bf16)
    down_own, *_ = lax.optimization_barrier((down_own, *[in_rows[x][0] for x in range(1, n_a)]))
    down_rows = fs_pieces(down_own, factors)

    normed = rms_rows(swap_gather(tokens, "tp", n_tp, 1), norm_gain)
    pool_in = (dot(normed, w_in_all) * scale_in).astype(bf16)
    pooled = pool_local(pool_in, lax.axis_index("tp") * pool_in.shape[1])
    pooled_all = swap_gather(pooled, "tp", n_tp, 1)
    groups = pool_w.shape[0]
    grouped = jnp.einsum(
        "lgc,gcd->lgd", pooled_all.reshape(length, groups, GROUP), pool_w, preferred_element_type=f32
    ).reshape(length, groups * GROUP).astype(bf16)
    mixed = (tokens.astype(f32) + dot(grouped, w_out_all) * scale_out).astype(bf16)

    mixed_own = swap_gather(mixed, "tp", n_tp, 1)
    sequences = [mixed_own]
    for offset in range(1, n_rep):
        other = shifted(mixed, "rep", n_rep, offset)
        sequences.append(swap_gather(other, "tp", n_tp, 1))
    scale_hidden = lax.dynamic_slice_in_dim(scale_up, rep * hidden_width, hidden_width, 0)
    hidden = []
    for rows in sequences:
        rows = rms_rows(rows, ffn_gain)
        upward = dot(rows, up_all)
        hidden.append(jnp.square(jax.nn.relu(upward * scale_hidden)).astype(bf16))

    hidden = jnp.concatenate(hidden, axis=0)
    width = w_down.shape[1]
    per_tp = n_a // n_tp
    tp = lax.axis_index("tp")
    turn = ((lax.axis_index("fs") // factors[1]) // per_tp) ^ tp
    result = jnp.zeros((length, local_width), bf16)
    for y in range(factors[1]):
        for xi in range(per_tp):
            stacked = jnp.stack([down_rows[xt * per_tp + xi][y] for xt in range(n_tp)])
            blocks, block_scales = [], []
            for k in range(n_tp):
                blocks.append(lax.dynamic_index_in_dim(stacked, turn ^ k, 0, keepdims=False))
                origin = fs_origin(factors, xi, y) ^ ((turn ^ k) * per_tp * factors[1])
                block_scales.append(lax.dynamic_index_in_dim(scale_down, origin, 0, keepdims=False))
            both = jnp.concatenate(blocks, axis=1)
            partial = (dot(hidden, both) * jnp.concatenate(block_scales)).astype(bf16)
            total = partial[:, :width].astype(f32)
            for k in range(1, n_tp):
                pairs = [(i, i ^ k) for i in range(n_tp)]
                total = total + lax.ppermute(partial[:, k * width:(k + 1) * width], "tp", pairs).astype(f32)
            own = total[:length]
            for k in range(1, n_rep):
                back = shifted(total[k * length:(k + 1) * length].astype(bf16), "rep", n_rep, -k)
                own = own + back.astype(f32)
            inner = (fs_origin(factors, xi, y) % (per_tp * factors[1])) * width
            mixed_part = lax.dynamic_slice_in_dim(mixed, inner, width, 1)
            piece = (mixed_part.astype(f32) + own).astype(bf16)
            result = lax.dynamic_update_slice_in_dim(result, piece, inner, 1)
    return result[None]


UP_TILE = (512, 512)
DOWN_ROWS = 512
MESH = pl.DeviceIdType.MESH
VMEM_BYTES = 67_043_328


def fused_kernel(
    n_fs, n_tp,
    stream, w_up, w_down, w_in, w_out, pool_w, norm_gain, ffn_gain, own_scales,
    out,
    up_all, down_all, up_other, down_other, ffn_rows, hidden, mixed, in_all, out_all,
    pool_in, grouped, squares, core_got, core_sent, pair_got, pair_sent, totals, pair_total,
    up_floats, scales, scale_in, scale_out, scale_up,
    load_sem, scale_send, scale_recv,
    mix_recv, mix_own_send, mix_z_send, mix_x_send, mix_y_send,
    piece_recv, own_send, z_send, x_send, y_send,
    core_send, core_recv, act_core_send, act_core_recv, act_pair_send, act_pair_recv,
    part_core_send, part_core_recv, part_pair_send, part_pair_recv, store_sem,
):
    rep, fs, tp = lax.axis_index("rep"), lax.axis_index("fs"), lax.axis_index("tp")
    n_z = n_fs // 2
    z, y = fs // 2, fs % 2
    length, local = stream.shape
    width = n_tp * local
    units = up_all.shape[1]
    block = down_all.shape[2]
    owned = n_fs // n_tp
    in_rows, out_rows = w_in.shape[0], w_out.shape[0]
    pool_width = pool_in.shape[1]
    core, across, pair = {"tp": 1 - tp}, {"rep": 1 - rep}, {"fs": fs + 1 - 2 * y}

    def remote(ref, there, sent, got, device):
        return pltpu.make_async_remote_copy(
            src_ref=ref, dst_ref=there, send_sem=sent, recv_sem=got,
            device_id=device, device_id_type=MESH,
        )

    def at_step(i):
        j, other = i // 2, i % 2
        both = jnp.minimum(z, n_z - 1 - z)
        paired = j <= 2 * both
        distance = jnp.where(paired, (j + 1) // 2, j - both)
        left = jnp.where(paired, j % 2 == 1, z > n_z - 1 - z)
        source = z + jnp.where(left, -distance, distance)
        return source * 2 + y + other - 2 * y * other, left

    def onward(left):
        return jnp.where(left, z < n_z - 1, z > 0), {"fs": fs + jnp.where(left, 2, -2)}

    def piece(kind, source, half):
        if kind == 0:
            rows = up_other.shape[0]
            return up_all.at[pl.ds(pl.multiple_of(source * rows + half * (rows // 2), rows // 2), rows // 2), :]
        return down_all.at[source, pl.ds(pl.multiple_of(half * (units // 2), units // 2), units // 2), :]

    def mix_piece(kind, source, half):
        ref, rows = ((in_all, in_rows), (out_all, out_rows))[kind]
        return ref.at[pl.ds(pl.multiple_of(source * rows + half * (rows // 2), rows // 2), rows // 2), :]

    def own_copy(kind, order, side):
        source = fs if order == 0 else fs + 1 - 2 * y
        ref = piece(kind, source, rep)
        return remote(ref, ref, own_send.at[kind, side, order], piece_recv.at[kind, source, rep],
                      {"fs": fs + (2 if side == 0 else -2)})

    def pair_copy(kind, half):
        if kind == 0:
            rows = up_other.shape[0] // 2
            ref = up_other.at[pl.ds(pl.multiple_of(half * rows, rows), rows), :]
        else:
            ref = down_other.at[pl.ds(pl.multiple_of(half * (units // 2), units // 2), units // 2), :]
        return remote(ref, piece(kind, fs, half), y_send.at[kind, half], piece_recv.at[kind, fs, half], pair)

    def onward_copy(kind, source, device):
        ref = piece(kind, source, rep)
        return remote(ref, ref, z_send.at[kind, source], piece_recv.at[kind, source, rep], device)

    def across_copy(kind, source):
        ref = piece(kind, source, rep)
        return remote(ref, ref, x_send.at[kind, source], piece_recv.at[kind, source, rep], across)

    def piece_wait(kind, source, half):
        ref = piece(kind, source, half)
        remote(ref, ref, x_send.at[kind, source], piece_recv.at[kind, source, half], across).wait_recv()

    def both_sides(act):
        @pl.when(z < n_z - 1)
        def _():
            act(0)

        @pl.when(z > 0)
        def _():
            act(1)

    def send_own(kind):
        both_sides(lambda side: own_copy(kind, 0, side).start())

    def send_pair(kind):
        for turn in range(2):
            pair_copy(kind, rep + turn - 2 * rep * turn).start()

    def pass_pair(kind):
        piece_wait(kind, fs + 1 - 2 * y, rep)
        both_sides(lambda side: own_copy(kind, 1, side).start())

    def pass_on(kind, i):
        source, left = at_step(i)
        piece_wait(kind, source, rep)
        going, device = onward(left)

        @pl.when(going)
        def _():
            onward_copy(kind, source, device).start()

        across_copy(kind, source).start()

    def mix_own_copy(kind, side):
        ref = mix_piece(kind, fs, rep)
        return remote(ref, ref, mix_own_send.at[kind, side], mix_recv.at[kind, fs, rep],
                      {"fs": fs + (2 if side == 0 else -2)})

    def mix_onward_copy(kind, source, device):
        ref = mix_piece(kind, source, rep)
        return remote(ref, ref, mix_z_send.at[kind, source], mix_recv.at[kind, source, rep], device)

    def mix_across_copy(kind, source):
        ref = mix_piece(kind, source, rep)
        return remote(ref, ref, mix_x_send.at[kind, source], mix_recv.at[kind, source, rep], across)

    def mix_pair_copy(kind, source, half):
        ref = mix_piece(kind, source, half)
        return remote(ref, ref, mix_y_send.at[kind, source, half], mix_recv.at[kind, source, half], pair)

    def mix_wait(kind, source, half):
        mix_pair_copy(kind, source, half).wait_recv()

    def scale_copy(offset):
        return remote(own_scales, scales.at[fs], scale_send.at[offset], scale_recv.at[fs],
                      {"fs": lax.rem(fs + offset, n_fs)})

    def core_copy(which, ref, there):
        return remote(ref, there, core_send.at[which], core_recv.at[which], core)

    my_half = pl.ds(pl.multiple_of(tp * local, local), local)
    my_pool = pl.ds(pl.multiple_of(tp * pool_width, pool_width), pool_width)
    n_tiles = 4
    tile = length // n_tiles

    def rows_of(t):
        return pl.ds(pl.multiple_of(t * tile, tile), tile)

    def act_pair_copy(t):
        return remote(ffn_rows.at[0, rows_of(t), my_half], ffn_rows.at[1, rows_of(t), my_half],
                      act_pair_send.at[t], act_pair_recv.at[t], pair)

    def act_core_copy(which, t):
        ref = ffn_rows.at[which, rows_of(t), my_half]
        return remote(ref, ref, act_core_send.at[which, t], act_core_recv.at[which, t], core)

    load_tokens = pltpu.make_async_copy(stream, mixed, load_sem.at[0])

    def load_up(which, half):
        return pltpu.make_async_copy(
            w_up.at[:, pl.ds(pl.multiple_of(half * units, units), units)], up_floats, load_sem.at[1 + which])

    quarter = units // 2

    def load_down(q):
        return pltpu.make_async_copy(
            w_down.at[pl.ds(q * quarter, quarter), :], totals.at[q], load_sem.at[3 + q])

    load_tokens.start()
    load_up(0, 1 - y).start()
    for q in range(4):
        load_down(q).start()

    own_in = pl.ds(pl.multiple_of(fs * in_rows, in_rows), in_rows)
    own_out = pl.ds(pl.multiple_of(fs * out_rows, out_rows), out_rows)
    in_all[own_in, :] = w_in[...].astype(bf16)
    out_all[own_out, :] = w_out[...].astype(bf16)

    barrier = pltpu.get_barrier_semaphore()
    for offset in range(1, n_fs):
        pl.semaphore_signal(barrier, inc=1, device_id={"fs": lax.rem(fs + offset, n_fs)}, device_id_type=MESH)
    pl.semaphore_signal(barrier, inc=1, device_id=across, device_id_type=MESH)
    pl.semaphore_signal(barrier, inc=1, device_id=core, device_id_type=MESH)
    pl.semaphore_wait(barrier, n_fs + 1)

    for kind in range(2):
        both_sides(lambda side, kind=kind: mix_own_copy(kind, side).start())
        for half in range(2):
            mix_pair_copy(kind, fs, half).start()
    for offset in range(1, n_fs):
        scale_copy(offset).start()
    scales[fs] = own_scales[...]

    load_tokens.wait()

    def square_rows(t, carry):
        floats = mixed[rows_of(t), :].astype(f32)
        total = jnp.sum(floats * floats, axis=1, keepdims=True)
        squares[0, rows_of(t), :] = jnp.broadcast_to(total, (tile, 128))
        return carry

    lax.fori_loop(0, n_tiles, square_rows, 0)
    share_squares = core_copy(0, squares.at[0], squares.at[1])
    share_squares.start()

    def mix_step(j):
        source, left = at_step(2 * j)
        going, device = onward(left)
        for kind in range(2):
            mix_wait(kind, source, rep)

            @pl.when(going)
            def _():
                mix_onward_copy(kind, source, device).start()

            mix_across_copy(kind, source).start()
            mix_pair_copy(kind, source, rep).start()

    load_up(0, 1 - y).wait()
    pieces = 8
    up_tile = up_floats.shape[0] // pieces

    def cast_other(t, carry):
        rows = pl.ds(pl.multiple_of(t * up_tile, up_tile), up_tile)
        up_other[rows, :] = up_floats[rows, :].astype(bf16)
        return carry

    lax.fori_loop(0, pieces, cast_other, 0)
    load_up(1, y).start()

    share_squares.wait()

    def normed_rows(t, carry):
        rows = rows_of(t)
        total = squares[0, rows, :] + squares[1, rows, :]
        scale = lax.rsqrt(total[:, :1] * (1.0 / width) + epsilon)
        floats = mixed[rows, :].astype(f32)
        hidden[1, rows, my_half] = (floats * scale * norm_gain[pl.ds(tp, 1), :]).astype(bf16)
        return carry

    lax.fori_loop(0, n_tiles, normed_rows, 0)
    share_normed = core_copy(1, hidden.at[1, :, my_half], hidden.at[1, :, my_half])
    share_normed.start()

    mix_step(1)

    load_up(1, y).wait()

    def cast_own(t, carry):
        rows = pl.ds(pl.multiple_of(t * up_tile, up_tile), up_tile)
        there = pl.ds(pl.multiple_of(fs * up_floats.shape[0] + t * up_tile, up_tile), up_tile)
        up_all[there, :] = up_floats[rows, :].astype(bf16)
        return carry

    lax.fori_loop(0, pieces, cast_own, 0)

    for j in range(2, n_z):
        mix_step(j)
    send_own(0)
    send_pair(0)

    for q in range(4):
        load_down(q).wait()
    down_tile = quarter // pieces

    def cast_down(t, carry):
        rows = pl.ds(pl.multiple_of(t * down_tile, down_tile), down_tile)
        for half in range(2):
            there = pl.ds(pl.multiple_of(half * quarter + t * down_tile, down_tile), down_tile)
            down_all[fs, there, :] = totals[2 * y + half, rows, :].astype(bf16)
            down_other[there, :] = totals[2 - 2 * y + half, rows, :].astype(bf16)
        return carry

    lax.fori_loop(0, pieces, cast_down, 0)

    for j in range(1, n_z):
        source, _ = at_step(2 * j)
        for kind in range(2):
            mix_wait(kind, source, 1 - rep)
            mix_pair_copy(kind, source, 1 - rep).start()
    send_own(1)

    for offset in range(1, n_fs):
        source = lax.rem(fs + offset, n_fs)
        remote(own_scales, scales.at[source], scale_send.at[offset], scale_recv.at[source], pair).wait_recv()
    gathered = scales[...]
    summed = jnp.sum(gathered[:, 0:2, :], axis=0)
    scale_in[...] = jnp.concatenate([summed[0:1], summed[1:2]], axis=1)
    for source in range(n_fs):
        scale_out[:, source * 128:(source + 1) * 128] = gathered[source, 2:3, :]
    per = units // (n_fs // 2)
    for q in range(n_fs // 2):
        rows = scales[y * (n_fs // 2) + q]
        for i in range(per // 128):
            scale_up[:, q * per + i * 128:q * per + (i + 1) * 128] = rows[3 + i:4 + i, :]

    for source_z in range(n_z):
        for kind in range(2):
            for half in range(2):
                mix_wait(kind, source_z * 2 + 1 - y, half)

    share_normed.wait()

    def pool_rows(t, carry):
        rows = rows_of(t)
        product = jnp.dot(hidden[1, rows, :], in_all[...], preferred_element_type=f32)
        pool_in[rows, :] = (product * scale_in[...]).astype(bf16)
        return carry

    lax.fori_loop(0, n_tiles, pool_rows, 0)
    pass_pair(0)
    per_core = pool_width // GROUP

    def group_rows(t, carry):
        rows = rows_of(t)
        target = lax.broadcasted_iota(jnp.int32, (tile, length), 0) + t * tile
        source = lax.broadcasted_iota(jnp.int32, (tile, length), 1)
        gap = source - target
        at = lax.broadcasted_iota(jnp.int32, (tile, GROUP), 0) + t * tile
        for g in range(per_core):
            half = jnp.left_shift(jnp.int32(1), tp * per_core + g)
            lanes = slice(g * GROUP, (g + 1) * GROUP)
            band = jnp.where((gap >= -half) & (gap < half), 1.0, 0.0).astype(bf16)
            sums = jnp.dot(band, pool_in[:, lanes], preferred_element_type=f32)
            counts = (jnp.minimum(at + half, length) - jnp.maximum(at - half, 0)).astype(f32)
            pooled = (sums / counts - pool_in[rows, lanes].astype(f32)).astype(bf16)
            product = jnp.dot(pooled, pool_w[tp * per_core + g], preferred_element_type=f32)
            there = pl.ds(pl.multiple_of(tp * pool_width + g * GROUP, GROUP), GROUP)
            grouped[rows, there] = product.astype(bf16)
        return carry

    lax.fori_loop(0, n_tiles, group_rows, 0)
    share_grouped = core_copy(2, grouped.at[:, my_pool], grouped.at[:, my_pool])
    share_grouped.start()
    pass_on(0, 2)
    share_grouped.wait()

    def mix_rows(t, carry):
        rows = rows_of(t)
        product = jnp.dot(grouped[rows, :], out_all[...], preferred_element_type=f32)
        total = (mixed[rows, :].astype(f32) + product * scale_out[...]).astype(bf16)
        mixed[rows, :] = total
        floats = total.astype(f32)
        squares[0, rows, :] = jnp.broadcast_to(jnp.sum(floats * floats, axis=1, keepdims=True), (tile, 128))
        return carry

    lax.fori_loop(0, n_tiles, mix_rows, 0)
    share_more = core_copy(3, squares.at[0], squares.at[1])
    share_more.start()
    share_more.wait()

    def ffn_in_rows(t, carry):
        rows = rows_of(t)
        total = squares[0, rows, :] + squares[1, rows, :]
        scale = lax.rsqrt(total[:, :1] * (1.0 / width) + epsilon)
        floats = mixed[rows, :].astype(f32)
        ffn_rows[0, rows, my_half] = (floats * scale * ffn_gain[pl.ds(tp, 1), :]).astype(bf16)
        act_pair_copy(t).start()
        act_core_copy(0, t).start()
        return carry

    lax.fori_loop(0, n_tiles, ffn_in_rows, 0)
    send_pair(1)

    for i in range(3, 2 * n_z):
        pass_on(0, i)
    piece_wait(0, fs + 1 - 2 * y, 1 - rep)

    def up_ready(i, carry):
        source, _ = at_step(i)
        piece_wait(0, source, 1 - rep)
        return carry

    lax.fori_loop(2, 2 * n_z, up_ready, 0)
    for t in range(n_tiles):
        act_core_copy(0, t).wait_recv()

    up_rows, up_columns = UP_TILE
    n_rows, n_columns = length // up_rows, units // up_columns

    def up_tiles(sequence):
        def body(n, carry):
            rows = pl.ds(pl.multiple_of((n % n_rows) * up_rows, up_rows), up_rows)
            columns = pl.ds(pl.multiple_of((n // n_rows) * up_columns, up_columns), up_columns)
            product = jnp.dot(ffn_rows[sequence, rows, :], up_all[:, columns], preferred_element_type=f32)
            positive = jnp.maximum(product * scale_up[:, columns], 0.0)
            hidden[sequence, rows, columns] = (positive * positive).astype(bf16)
            return carry

        return body

    pass_pair(1)
    lax.fori_loop(0, n_rows * n_columns, up_tiles(0), 0)
    for t in range(n_tiles):
        act_pair_copy(t).wait_recv()
        act_core_copy(1, t).start()
    pass_on(1, 2)
    for t in range(n_tiles):
        act_core_copy(1, t).wait_recv()
    lax.fori_loop(0, n_rows * n_columns // 2, up_tiles(1), 0)
    pass_on(1, 3)
    lax.fori_loop(n_rows * n_columns // 2, n_rows * n_columns, up_tiles(1), 0)

    down_rows = DOWN_ROWS

    def part_core_copy(index, sequence):
        span = pl.ds(sequence * length, length)
        return remote(core_sent.at[index, span, :], core_got.at[index, span, :],
                      part_core_send.at[index, sequence], part_core_recv.at[index, sequence], core)

    def part_pair_copy(index):
        return remote(pair_sent.at[index], pair_got.at[index],
                      part_pair_send.at[index], part_pair_recv.at[index], pair)

    def down_block(i, carry):
        @pl.when((i >= 3) & (i < 2 * n_z - 1))
        def _():
            pass_on(1, i + 1)

        source, _ = at_step(i)

        @pl.when(i > 0)
        def _():
            piece_wait(1, source, 1 - rep)

        index = source % owned
        mine = source // owned == tp
        scale = jnp.concatenate([scales[source, 7:8, :], scales[source, 8:9, :]], axis=1)
        for sequence in (1, 0):
            def down_tile_rows(m, inner):
                rows = pl.ds(pl.multiple_of(m * down_rows, down_rows), down_rows)
                product = jnp.dot(hidden[sequence, rows, :], down_all[source], preferred_element_type=f32) * scale

                @pl.when(mine)
                def _():
                    if sequence == 1:
                        pair_total[rows, :] = product
                    else:
                        totals[index, rows, :] = product

                @pl.when(jnp.logical_not(mine))
                def _():
                    there = pl.ds(pl.multiple_of(sequence * length + m * down_rows, down_rows), down_rows)
                    core_sent[index, there, :] = product.astype(bf16)

                return inner

            lax.fori_loop(0, length // down_rows, down_tile_rows, 0)

            @pl.when(jnp.logical_not(mine))
            def _():
                part_core_copy(index, sequence).start()

        @pl.when(mine)
        def _():
            part_core_copy(index, 1).wait_recv()
            pair_sent[index] = (pair_total[...] + core_got[index, length:2 * length, :].astype(f32)).astype(bf16)
            part_pair_copy(index).start()

        return carry

    lax.fori_loop(0, n_fs, down_block, 0)

    def store_block(index):
        columns = pl.ds(pl.multiple_of(index * block, block), block)
        return pltpu.make_async_copy(pair_sent.at[index], out.at[:, columns], store_sem.at[index])

    def finish_block(i, carry):
        source, _ = at_step(i)

        @pl.when(source // owned == tp)
        def _():
            index = source % owned
            columns = pl.ds(pl.multiple_of(index * block, block), block)
            part_core_copy(index, 0).wait_recv()
            part_pair_copy(index).wait()
            total = totals[index] + core_got[index, 0:length, :].astype(f32) + pair_got[index].astype(f32)
            pair_sent[index] = (mixed[:, columns].astype(f32) + total).astype(bf16)
            store_block(index).start()

        return carry

    lax.fori_loop(0, n_fs, finish_block, 0)

    for kind in range(2):
        both_sides(lambda side, kind=kind: mix_own_copy(kind, side).wait_send())
        for order in range(2):
            both_sides(lambda side, kind=kind, order=order: own_copy(kind, order, side).wait_send())
        for half in range(2):
            mix_pair_copy(kind, fs, half).wait_send()
            pair_copy(kind, half).wait_send()

        def sent_step(i, carry, kind=kind):
            source, left = at_step(i)
            going, device = onward(left)

            @pl.when(going)
            def _():
                onward_copy(kind, source, device).wait_send()

            across_copy(kind, source).wait_send()

            @pl.when(i % 2 == 0)
            def _():
                @pl.when(going)
                def _():
                    mix_onward_copy(kind, source, device).wait_send()

                mix_across_copy(kind, source).wait_send()
                mix_pair_copy(kind, source, 0).wait_send()
                mix_pair_copy(kind, source, 1).wait_send()

            return carry

        lax.fori_loop(2, 2 * n_z, sent_step, 0)
    for offset in range(1, n_fs):
        scale_copy(offset).wait_send()
    for t in range(n_tiles):
        act_pair_copy(t).wait_send()
        for which in range(2):
            act_core_copy(which, t).wait_send()
    for index in range(owned):
        for sequence in range(2):
            part_core_copy(index, sequence).wait_send()
        store_block(index).wait()


def fused(n_fs, n_tp, stream, norm_gain, w_in, s_in, pool_w, w_out, s_out,
          ffn_gain, w_up, s_up, w_down, s_down):
    fs = lax.axis_index("fs")
    tokens = stream[0]
    length, local = tokens.shape
    rows, all_units = w_up.shape
    units = all_units // 2
    block = w_down.shape[1]
    in_rows, pool_width = w_in.shape
    out_rows = w_out.shape[0]
    owned = n_fs // n_tp
    placed_in = lax.dynamic_update_slice(jnp.zeros((pool_width,), f32), s_in, (fs * s_in.shape[0],))
    packed = jnp.concatenate([placed_in, s_out, s_up, s_down])
    packed = jnp.pad(packed, (0, 16 * 128 - packed.shape[0])).reshape(16, 128)
    vmem, anywhere = pl.BlockSpec(memory_space=pltpu.VMEM), pl.BlockSpec(memory_space=pl.ANY)
    dma = pltpu.SemaphoreType.DMA
    result = pl.pallas_call(
        functools.partial(fused_kernel, n_fs, n_tp),
        out_shape=jax.ShapeDtypeStruct((length, local), bf16),
        in_specs=[anywhere] * 3 + [vmem] * 6,
        out_specs=anywhere,
        scratch_shapes=[
            pltpu.VMEM((rows * n_fs, units), bf16),
            pltpu.VMEM((n_fs, units, block), bf16),
            pltpu.VMEM((rows, units), bf16),
            pltpu.VMEM((units, block), bf16),
            pltpu.VMEM((2, length, n_tp * local), bf16),
            pltpu.VMEM((2, length, units), bf16),
            pltpu.VMEM((length, local), bf16),
            pltpu.VMEM((in_rows * n_fs, pool_width), bf16),
            pltpu.VMEM((out_rows * n_fs, local), bf16),
            pltpu.VMEM((length, pool_width), bf16),
            pltpu.VMEM((length, n_tp * pool_width), bf16),
            pltpu.VMEM((2, length, 128), f32),
            pltpu.VMEM((owned, 2 * length, block), bf16),
            pltpu.VMEM((owned, 2 * length, block), bf16),
            pltpu.VMEM((owned, length, block), bf16),
            pltpu.VMEM((owned, length, block), bf16),
            pltpu.VMEM((owned, length, block), f32),
            pltpu.VMEM((length, block), f32),
            pltpu.VMEM((rows, units), f32),
            pltpu.VMEM((n_fs, 16, 128), f32),
            pltpu.VMEM((1, pool_width), f32),
            pltpu.VMEM((1, local), f32),
            pltpu.VMEM((1, units), f32),
            dma((7,)), dma((n_fs,)), dma((n_fs,)),
            dma((2, n_fs, 2)), dma((2, 2)), dma((2, n_fs)), dma((2, n_fs)), dma((2, n_fs, 2)),
            dma((2, n_fs, 2)), dma((2, 2, 2)), dma((2, n_fs)), dma((2, n_fs)), dma((2, 2)),
            dma((4,)), dma((4,)), dma((2, 4)), dma((2, 4)), dma((4,)), dma((4,)),
            dma((owned, 2)), dma((owned, 2)), dma((owned,)), dma((owned,)), dma((owned,)),
        ],
        compiler_params=pltpu.CompilerParams(
            collective_id=0, has_side_effects=True, vmem_limit_bytes=VMEM_BYTES
        ),
        name="fused_layer",
    )(tokens, w_up, w_down, w_in, w_out, pool_w,
      norm_gain.reshape(n_tp, local), ffn_gain.reshape(n_tp, local), packed)
    return result[None]


def fits(n_rep, n_fs, n_tp, args):
    stream, w_in, pool_w, w_down = args[0], args[2], args[4], args[10]
    return (
        n_rep == 2 and n_tp == 2 and n_fs % 4 == 0
        and stream.shape[0] == 1
        and pool_w.shape[0] * GROUP == w_in.shape[1] * n_tp
        and stream.shape[2] * n_tp == w_down.shape[1] * n_fs
    )


def solution(mesh):
    n_rep, n_fs, n_tp = (mesh.shape[name] for name in ("rep", "fs", "tp"))

    def body(*args):
        if fits(n_rep, n_fs, n_tp, args):
            return fused(n_fs, n_tp, *args)
        return on_device(n_rep, n_fs, n_tp, *args)

    return jax.shard_map(
        body,
        mesh=mesh,
        in_specs=(
            P(("rep", "fs"), None, "tp"),
            P(),
            P("fs", "tp"),
            P(("tp", "fs")),
            P(),
            P("fs", "tp"),
            P(("tp", "fs")),
            P(),
            P("fs", "tp"),
            P(("tp", "fs")),
            P("tp", "fs"),
            P("fs"),
        ),
        out_specs=P(("rep", "fs"), None, "tp"),
        check_vma=False,
    )
```

profile of v0, /device:TPU:1, one launch (start us, length us, event | category | flops | bytes accessed | tf_op | source)
XLA Modules:
  0.0 241.2 jit_solution(3811077200613915799)
XLA Ops:
  0.0 0.8 dynamic_update_slice.3
  0.8 1.3 fusion.own_scales
  2.1 1.3 reshape.9.norm_gain
  3.4 1.3 reshape.10.ffn_gain
  4.7 233.4 %fused_layer.1 = bf16[1024,1024]{1,0:T(8,128)(2,1)} custom-call(bf16[1024,1024]{1,0:T(8,128)(2,1)} %bitcast.5, f32[256,4096]{1,0:T(8,128)} %w_up.1, f32[4096,256]{1,0:T(8,128)} %w_down.1, f32[256,256]{1,0:T(8,128)} %w_in.1, f32[64,1024]{1,0:T(8,128)} %w_out.1, bf16[4,128,128]{2,1,0:T(8,128)(2,1)} %pool_w.1, f32[2,1024]{1,0:T(2,128)} %reshape.9.norm_gain, ...), custom_call_target="tpu_custom_call" | custom-call | tf_op jit(solution)/shard_map/fused_layer/pallas_call | solution.py:739
  238.1 3.1 %copy.15 = bf16[1,1024,1024]{2,1,0:T(8,128)(2,1)} copy(bf16[1,1024,1024]{2,1,0:T(8,128)(2,1)} %bitcast.4) | data formatting | bytes 4194304
  (1 shorter events, 0.0 us)
where the time goes:
time: 241 us
  Pallas kernels  233 us (97%)
  local copies, waits for them, and re-layouts  6.52 us (3%)
    pallas_call x1, Pallas kernels, fused(): pl.pallas_call(functools.partial(fused_kernel, n_fs, n_tp), out_shape=jax...  233 us

commit v1 on v0

--- a/solution.py
+++ b/solution.py
@@ -192,6 +192,7 @@
 
 UP_TILE = (512, 512)
 DOWN_ROWS = 512
+PARTS = 2
 MESH = pl.DeviceIdType.MESH
 VMEM_BYTES = 67_043_328
 
@@ -239,41 +240,45 @@
     def onward(left):
         return jnp.where(left, z < n_z - 1, z > 0), {"fs": fs + jnp.where(left, 2, -2)}
 
-    def piece(kind, source, half):
+    up_piece, down_piece = up_other.shape[0] // (2 * PARTS), units // (2 * PARTS)
+
+    def piece(kind, source, half, q):
+        place = half * PARTS + q
         if kind == 0:
-            rows = up_other.shape[0]
-            return up_all.at[pl.ds(pl.multiple_of(source * rows + half * (rows // 2), rows // 2), rows // 2), :]
-        return down_all.at[source, pl.ds(pl.multiple_of(half * (units // 2), units // 2), units // 2), :]
+            start = (source * 2 * PARTS + place) * up_piece
+            return up_all.at[pl.ds(pl.multiple_of(start, up_piece), up_piece), :]
+        return down_all.at[source, pl.ds(pl.multiple_of(place * down_piece, down_piece), down_piece), :]
 
     def mix_piece(kind, source, half):
         ref, rows = ((in_all, in_rows), (out_all, out_rows))[kind]
         return ref.at[pl.ds(pl.multiple_of(source * rows + half * (rows // 2), rows // 2), rows // 2), :]
 
-    def own_copy(kind, order, side):
+    def own_copy(kind, order, side, q):
         source = fs if order == 0 else fs + 1 - 2 * y
-        ref = piece(kind, source, rep)
-        return remote(ref, ref, own_send.at[kind, side, order], piece_recv.at[kind, source, rep],
+        ref = piece(kind, source, rep, q)
+        return remote(ref, ref, own_send.at[kind, side, order, q], piece_recv.at[kind, source, rep, q],
                       {"fs": fs + (2 if side == 0 else -2)})
 
-    def pair_copy(kind, half):
-        if kind == 0:
-            rows = up_other.shape[0] // 2
-            ref = up_other.at[pl.ds(pl.multiple_of(half * rows, rows), rows), :]
-        else:
-            ref = down_other.at[pl.ds(pl.multiple_of(half * (units // 2), units // 2), units // 2), :]
-        return remote(ref, piece(kind, fs, half), y_send.at[kind, half], piece_recv.at[kind, fs, half], pair)
-
-    def onward_copy(kind, source, device):
-        ref = piece(kind, source, rep)
-        return remote(ref, ref, z_send.at[kind, source], piece_recv.at[kind, source, rep], device)
-
-    def across_copy(kind, source):
-        ref = piece(kind, source, rep)
-        return remote(ref, ref, x_send.at[kind, source], piece_recv.at[kind, source, rep], across)
-
-    def piece_wait(kind, source, half):
-        ref = piece(kind, source, half)
-        remote(ref, ref, x_send.at[kind, source], piece_recv.at[kind, source, half], across).wait_recv()
+    def pair_copy(kind, half, q):
+        size = (up_piece, down_piece)[kind]
+        ref = (up_other, down_other)[kind].at[pl.ds(pl.multiple_of((half * PARTS + q) * size, size), size), :]
+        return remote(ref, piece(kind, fs, half, q), y_send.at[kind, half, q], piece_recv.at[kind, fs, half, q], pair)
+
+    def onward_copy(kind, source, q, device):
+        ref = piece(kind, source, rep, q)
+        return remote(ref, ref, z_send.at[kind, source, q], piece_recv.at[kind, source, rep, q], device)
+
+    def across_copy(kind, source, q):
+        ref = piece(kind, source, rep, q)
+        return remote(ref, ref, x_send.at[kind, source, q], piece_recv.at[kind, source, rep, q], across)
+
+    def piece_wait(kind, source, half, q):
+        ref = piece(kind, source, half, q)
+        remote(ref, ref, x_send.at[kind, source, q], piece_recv.at[kind, source, half, q], across).wait_recv()
+
+    def other_half(kind, source):
+        for q in range(PARTS):
+            piece_wait(kind, source, 1 - rep, q)
 
     def both_sides(act):
         @pl.when(z < n_z - 1)
@@ -284,27 +289,30 @@
         def _():
             act(1)
 
-    def send_own(kind):
-        both_sides(lambda side: own_copy(kind, 0, side).start())
+    def send_own(kind, q):
+        both_sides(lambda side: own_copy(kind, 0, side, q).start())
 
     def send_pair(kind):
         for turn in range(2):
-            pair_copy(kind, rep + turn - 2 * rep * turn).start()
+            for q in range(PARTS):
+                pair_copy(kind, rep + turn - 2 * rep * turn, q).start()
 
     def pass_pair(kind):
-        piece_wait(kind, fs + 1 - 2 * y, rep)
-        both_sides(lambda side: own_copy(kind, 1, side).start())
+        for q in range(PARTS):
+            piece_wait(kind, fs + 1 - 2 * y, rep, q)
+            both_sides(lambda side, q=q: own_copy(kind, 1, side, q).start())
 
     def pass_on(kind, i):
         source, left = at_step(i)
-        piece_wait(kind, source, rep)
         going, device = onward(left)
-
-        @pl.when(going)
-        def _():
-            onward_copy(kind, source, device).start()
-
-        across_copy(kind, source).start()
+        for q in range(PARTS):
+            piece_wait(kind, source, rep, q)
+
+            @pl.when(going)
+            def _():
+                onward_copy(kind, source, q, device).start()
+
+            across_copy(kind, source, q).start()
 
     def mix_own_copy(kind, side):
         ref = mix_piece(kind, fs, rep)
@@ -362,7 +370,7 @@
             w_down.at[pl.ds(q * quarter, quarter), :], totals.at[q], load_sem.at[3 + q])
 
     load_tokens.start()
-    load_up(0, 1 - y).start()
+    load_up(0, y).start()
     for q in range(4):
         load_down(q).start()
 
@@ -376,6 +384,32 @@
         pl.semaphore_signal(barrier, inc=1, device_id={"fs": lax.rem(fs + offset, n_fs)}, device_id_type=MESH)
     pl.semaphore_signal(barrier, inc=1, device_id=across, device_id_type=MESH)
     pl.semaphore_signal(barrier, inc=1, device_id=core, device_id_type=MESH)
+
+    pieces = 8
+    up_tile = up_floats.shape[0] // pieces
+
+    def cast_own(t, carry):
+        rows = pl.ds(pl.multiple_of(t * up_tile, up_tile), up_tile)
+        there = pl.ds(pl.multiple_of(fs * up_floats.shape[0] + t * up_tile, up_tile), up_tile)
+        up_all[there, :] = up_floats[rows, :].astype(bf16)
+        return carry
+
+    def cast_other(t, carry):
+        rows = pl.ds(pl.multiple_of(t * up_tile, up_tile), up_tile)
+        up_other[rows, :] = up_floats[rows, :].astype(bf16)
+        return carry
+
+    def square_rows(t, carry):
+        floats = mixed[rows_of(t), :].astype(f32)
+        total = jnp.sum(floats * floats, axis=1, keepdims=True)
+        squares[0, rows_of(t), :] = jnp.broadcast_to(total, (tile, 128))
+        return carry
+
+    load_up(0, y).wait()
+    lax.fori_loop(0, pieces, cast_own, 0)
+    load_up(1, 1 - y).start()
+    load_tokens.wait()
+    lax.fori_loop(0, n_tiles, square_rows, 0)
     pl.semaphore_wait(barrier, n_fs + 1)
 
     for kind in range(2):
@@ -384,19 +418,9 @@
             mix_pair_copy(kind, fs, half).start()
     for offset in range(1, n_fs):
         scale_copy(offset).start()
-    scales[fs] = own_scales[...]
-
-    load_tokens.wait()
-
-    def square_rows(t, carry):
-        floats = mixed[rows_of(t), :].astype(f32)
-        total = jnp.sum(floats * floats, axis=1, keepdims=True)
-        squares[0, rows_of(t), :] = jnp.broadcast_to(total, (tile, 128))
-        return carry
-
-    lax.fori_loop(0, n_tiles, square_rows, 0)
     share_squares = core_copy(0, squares.at[0], squares.at[1])
     share_squares.start()
+    scales[fs] = own_scales[...]
 
     def mix_step(j):
         source, left = at_step(2 * j)
@@ -411,18 +435,8 @@
             mix_across_copy(kind, source).start()
             mix_pair_copy(kind, source, rep).start()
 
-    load_up(0, 1 - y).wait()
-    pieces = 8
-    up_tile = up_floats.shape[0] // pieces
-
-    def cast_other(t, carry):
-        rows = pl.ds(pl.multiple_of(t * up_tile, up_tile), up_tile)
-        up_other[rows, :] = up_floats[rows, :].astype(bf16)
-        return carry
-
+    load_up(1, 1 - y).wait()
     lax.fori_loop(0, pieces, cast_other, 0)
-    load_up(1, y).start()
-
     share_squares.wait()
 
     def normed_rows(t, carry):
@@ -437,22 +451,10 @@
     share_normed = core_copy(1, hidden.at[1, :, my_half], hidden.at[1, :, my_half])
     share_normed.start()
 
-    mix_step(1)
-
-    load_up(1, y).wait()
-
-    def cast_own(t, carry):
-        rows = pl.ds(pl.multiple_of(t * up_tile, up_tile), up_tile)
-        there = pl.ds(pl.multiple_of(fs * up_floats.shape[0] + t * up_tile, up_tile), up_tile)
-        up_all[there, :] = up_floats[rows, :].astype(bf16)
-        return carry
-
-    lax.fori_loop(0, pieces, cast_own, 0)
-
-    for j in range(2, n_z):
+    for j in range(1, n_z):
         mix_step(j)
-    send_own(0)
-    send_pair(0)
+    for q in range(PARTS):
+        send_own(0, q)
 
     for q in range(4):
         load_down(q).wait()
@@ -466,14 +468,29 @@
             down_other[there, :] = totals[2 - 2 * y + half, rows, :].astype(bf16)
         return carry
 
-    lax.fori_loop(0, pieces, cast_down, 0)
+    inner = jnp.minimum(z, n_z - 1 - z) > 0
+
+    def inner_pass(kind, i):
+        @pl.when(inner)
+        def _():
+            pass_on(kind, i)
+
+    def outer_pass(kind, i):
+        @pl.when(jnp.logical_not(inner))
+        def _():
+            pass_on(kind, i)
 
     for j in range(1, n_z):
         source, _ = at_step(2 * j)
         for kind in range(2):
             mix_wait(kind, source, 1 - rep)
             mix_pair_copy(kind, source, 1 - rep).start()
-    send_own(1)
+    send_pair(0)
+    lax.fori_loop(0, pieces, cast_down, 0)
+    for q in range(PARTS):
+        send_own(1, q)
+    pass_on(0, 2)
+    inner_pass(0, 4)
 
     for offset in range(1, n_fs):
         source = lax.rem(fs + offset, n_fs)
@@ -503,7 +520,6 @@
         return carry
 
     lax.fori_loop(0, n_tiles, pool_rows, 0)
-    pass_pair(0)
     per_core = pool_width // GROUP
 
     def group_rows(t, carry):
@@ -527,7 +543,8 @@
     lax.fori_loop(0, n_tiles, group_rows, 0)
     share_grouped = core_copy(2, grouped.at[:, my_pool], grouped.at[:, my_pool])
     share_grouped.start()
-    pass_on(0, 2)
+    outer_pass(1, 2)
+    pass_pair(0)
     share_grouped.wait()
 
     def mix_rows(t, carry):
@@ -542,6 +559,8 @@
     lax.fori_loop(0, n_tiles, mix_rows, 0)
     share_more = core_copy(3, squares.at[0], squares.at[1])
     share_more.start()
+    inner_pass(0, 6)
+    outer_pass(0, 4)
     share_more.wait()
 
     def ffn_in_rows(t, carry):
@@ -557,13 +576,18 @@
     lax.fori_loop(0, n_tiles, ffn_in_rows, 0)
     send_pair(1)
 
-    for i in range(3, 2 * n_z):
-        pass_on(0, i)
-    piece_wait(0, fs + 1 - 2 * y, 1 - rep)
+    pass_on(0, 3)
+    outer_pass(0, 6)
+    pass_on(0, 5)
+    pass_on(0, 7)
+    inner_pass(1, 2)
+    inner_pass(1, 4)
+    inner_pass(1, 6)
+    other_half(0, fs + 1 - 2 * y)
 
     def up_ready(i, carry):
         source, _ = at_step(i)
-        piece_wait(0, source, 1 - rep)
+        other_half(0, source)
         return carry
 
     lax.fori_loop(2, 2 * n_z, up_ready, 0)
@@ -572,6 +596,7 @@
 
     up_rows, up_columns = UP_TILE
     n_rows, n_columns = length // up_rows, units // up_columns
+    half_tiles = n_rows * n_columns // 2
 
     def up_tiles(sequence):
         def body(n, carry):
@@ -584,17 +609,18 @@
 
         return body
 
-    pass_pair(1)
-    lax.fori_loop(0, n_rows * n_columns, up_tiles(0), 0)
     for t in range(n_tiles):
         act_pair_copy(t).wait_recv()
         act_core_copy(1, t).start()
-    pass_on(1, 2)
+    lax.fori_loop(0, half_tiles, up_tiles(0), 0)
+    outer_pass(1, 4)
+    lax.fori_loop(half_tiles, 2 * half_tiles, up_tiles(0), 0)
+    pass_pair(1)
     for t in range(n_tiles):
         act_core_copy(1, t).wait_recv()
-    lax.fori_loop(0, n_rows * n_columns // 2, up_tiles(1), 0)
-    pass_on(1, 3)
-    lax.fori_loop(n_rows * n_columns // 2, n_rows * n_columns, up_tiles(1), 0)
+    lax.fori_loop(0, half_tiles, up_tiles(1), 0)
+    outer_pass(1, 6)
+    lax.fori_loop(half_tiles, 2 * half_tiles, up_tiles(1), 0)
 
     down_rows = DOWN_ROWS
 
@@ -607,16 +633,27 @@
         return remote(pair_sent.at[index], pair_got.at[index],
                       part_pair_send.at[index], part_pair_recv.at[index], pair)
 
-    def down_block(i, carry):
-        @pl.when((i >= 3) & (i < 2 * n_z - 1))
-        def _():
-            pass_on(1, i + 1)
-
-        source, _ = at_step(i)
-
-        @pl.when(i > 0)
-        def _():
-            piece_wait(1, source, 1 - rep)
+    def down_order(n):
+        return jnp.where(n < n_z, 2 * n, 2 * (n - n_z) + 1)
+
+    def down_block(n, carry):
+        @pl.when(inner & (n >= 1) & (n < n_z - 1))
+        def _():
+            pass_on(1, 2 * n + 1)
+
+        @pl.when(jnp.logical_not(inner) & (n % 2 == 1) & (n < 2 * n_z - 4))
+        def _():
+            pass_on(1, n + 2)
+
+        @pl.when(n == 2 * n_z - 3)
+        def _():
+            pass_on(1, 2 * n_z - 1)
+
+        source, _ = at_step(down_order(n))
+
+        @pl.when(n > 0)
+        def _():
+            other_half(1, source)
 
         index = source % owned
         mine = source // owned == tp
@@ -661,7 +698,7 @@
         return pltpu.make_async_copy(pair_sent.at[index], out.at[:, columns], store_sem.at[index])
 
     def finish_block(i, carry):
-        source, _ = at_step(i)
+        source, _ = at_step(down_order(i))
 
         @pl.when(source // owned == tp)
         def _():
@@ -679,21 +716,24 @@
 
     for kind in range(2):
         both_sides(lambda side, kind=kind: mix_own_copy(kind, side).wait_send())
-        for order in range(2):
-            both_sides(lambda side, kind=kind, order=order: own_copy(kind, order, side).wait_send())
+        for q in range(PARTS):
+            for order in range(2):
+                both_sides(lambda side, kind=kind, order=order, q=q: own_copy(kind, order, side, q).wait_send())
+            for half in range(2):
+                pair_copy(kind, half, q).wait_send()
         for half in range(2):
             mix_pair_copy(kind, fs, half).wait_send()
-            pair_copy(kind, half).wait_send()
 
         def sent_step(i, carry, kind=kind):
             source, left = at_step(i)
             going, device = onward(left)
 
-            @pl.when(going)
-            def _():
-                onward_copy(kind, source, device).wait_send()
-
-            across_copy(kind, source).wait_send()
+            for q in range(PARTS):
+                @pl.when(going)
+                def _():
+                    onward_copy(kind, source, q, device).wait_send()
+
+                across_copy(kind, source, q).wait_send()
 
             @pl.when(i % 2 == 0)
             def _():
@@ -767,7 +807,8 @@
             pltpu.VMEM((1, units), f32),
             dma((7,)), dma((n_fs,)), dma((n_fs,)),
             dma((2, n_fs, 2)), dma((2, 2)), dma((2, n_fs)), dma((2, n_fs)), dma((2, n_fs, 2)),
-            dma((2, n_fs, 2)), dma((2, 2, 2)), dma((2, n_fs)), dma((2, n_fs)), dma((2, 2)),
+            dma((2, n_fs, 2, PARTS)), dma((2, 2, 2, PARTS)), dma((2, n_fs, PARTS)), dma((2, n_fs, PARTS)),
+            dma((2, 2, PARTS)),
             dma((4,)), dma((4,)), dma((2, 4)), dma((2, 4)), dma((4,)), dma((4,)),
             dma((owned, 2)), dma((owned, 2)), dma((owned,)), dma((owned,)), dma((owned,)),
         ],

time: 241 us -> 191 us (0.79)
  Pallas kernels: 233 us -> 183 us
    pallas_call x1, Pallas kernels: 233 us -> 183 us  [fused(): pl.pallas_call(functools.partial(fused_kernel, n_fs, n_tp), out_shape=jax...]
where the time goes in v1:
time: 191 us
  Pallas kernels  183 us (96%)
  local copies, waits for them, and re-layouts  6.52 us (3%)
    pallas_call x1, Pallas kernels, fused(): pl.pallas_call(functools.partial(fused_kernel, n_fs, n_tp), out_shape=jax...  183 us

profile of v1, /device:TPU:1, one launch (start us, length us, event | category | flops | bytes accessed | tf_op | source)
XLA Modules:
  0.0 190.5 jit_solution(13290821423518770863)
XLA Ops:
  0.0 0.8 dynamic_update_slice.3
  0.8 1.3 fusion.own_scales
  2.1 1.3 reshape.9.norm_gain
  3.4 1.3 reshape.10.ffn_gain
  4.7 182.7 %fused_layer.1 = bf16[1024,1024]{1,0:T(8,128)(2,1)} custom-call(bf16[1024,1024]{1,0:T(8,128)(2,1)} %bitcast.5, f32[256,4096]{1,0:T(8,128)} %w_up.1, f32[4096,256]{1,0:T(8,128)} %w_down.1, f32[256,256]{1,0:T(8,128)} %w_in.1, f32[64,1024]{1,0:T(8,128)} %w_out.1, bf16[4,128,128]{2,1,0:T(8,128)(2,1)} %pool_w.1, f32[2,1024]{1,0:T(2,128)} %reshape.9.norm_gain, ...), custom_call_target="tpu_custom_call" | custom-call | tf_op jit(solution)/shard_map/fused_layer/pallas_call | solution.py:779
  187.5 3.1 %copy.15 = bf16[1,1024,1024]{2,1,0:T(8,128)(2,1)} copy(bf16[1,1024,1024]{2,1,0:T(8,128)(2,1)} %bitcast.4) | data formatting | bytes 4194304
  (1 shorter events, 0.0 us)

commit v2 on v1

--- a/solution.py
+++ b/solution.py
@@ -190,6 +190,7 @@
     return result[None]
 
 
+LANES = 128
 UP_TILE = (512, 512)
 DOWN_ROWS = 512
 PARTS = 2
@@ -199,11 +200,11 @@
 
 def fused_kernel(
     n_fs, n_tp,
-    stream, w_up, w_down, w_in, w_out, pool_w, norm_gain, ffn_gain, own_scales,
+    stream, w_up, w_down, w_in, w_out, pool_w, norm_gain, ffn_gain, s_in, s_out, s_up, s_down,
     out,
     up_all, down_all, up_other, down_other, ffn_rows, hidden, mixed, in_all, out_all,
     pool_in, grouped, squares, core_got, core_sent, pair_got, pair_sent, totals, pair_total,
-    up_floats, scales, scale_in, scale_out, scale_up,
+    up_floats, own_scales, scales, scale_in, scale_out, scale_up,
     load_sem, scale_send, scale_recv,
     mix_recv, mix_own_send, mix_z_send, mix_x_send, mix_y_send,
     piece_recv, own_send, z_send, x_send, y_send,
@@ -379,6 +380,15 @@
     in_all[own_in, :] = w_in[...].astype(bf16)
     out_all[own_out, :] = w_out[...].astype(bf16)
 
+    up_lines, down_lines = s_up.shape[1] // LANES, block // LANES
+    own_scales[0:1, 0:s_in.shape[1]] = s_in[...]
+    own_scales[1:2, :] = s_out[...]
+    for i in range(up_lines):
+        own_scales[2 + i:3 + i, :] = s_up[:, i * LANES:(i + 1) * LANES]
+    for i in range(down_lines):
+        line = 2 + up_lines + i
+        own_scales[line:line + 1, :] = s_down[:, i * LANES:(i + 1) * LANES]
+
     barrier = pltpu.get_barrier_semaphore()
     for offset in range(1, n_fs):
         pl.semaphore_signal(barrier, inc=1, device_id={"fs": lax.rem(fs + offset, n_fs)}, device_id_type=MESH)
@@ -402,7 +412,7 @@
     def square_rows(t, carry):
         floats = mixed[rows_of(t), :].astype(f32)
         total = jnp.sum(floats * floats, axis=1, keepdims=True)
-        squares[0, rows_of(t), :] = jnp.broadcast_to(total, (tile, 128))
+        squares[0, rows_of(t), :] = jnp.broadcast_to(total, (tile, LANES))
         return carry
 
     load_up(0, y).wait()
@@ -444,7 +454,7 @@
         total = squares[0, rows, :] + squares[1, rows, :]
         scale = lax.rsqrt(total[:, :1] * (1.0 / width) + epsilon)
         floats = mixed[rows, :].astype(f32)
-        hidden[1, rows, my_half] = (floats * scale * norm_gain[pl.ds(tp, 1), :]).astype(bf16)
+        hidden[1, rows, my_half] = (floats * scale * norm_gain[:, my_half]).astype(bf16)
         return carry
 
     lax.fori_loop(0, n_tiles, normed_rows, 0)
@@ -495,16 +505,15 @@
     for offset in range(1, n_fs):
         source = lax.rem(fs + offset, n_fs)
         remote(own_scales, scales.at[source], scale_send.at[offset], scale_recv.at[source], pair).wait_recv()
-    gathered = scales[...]
-    summed = jnp.sum(gathered[:, 0:2, :], axis=0)
-    scale_in[...] = jnp.concatenate([summed[0:1], summed[1:2]], axis=1)
+    few = s_in.shape[1]
     for source in range(n_fs):
-        scale_out[:, source * 128:(source + 1) * 128] = gathered[source, 2:3, :]
-    per = units // (n_fs // 2)
+        scale_in[:, source * few:(source + 1) * few] = scales[source, 0:1, 0:few]
+        scale_out[:, source * LANES:(source + 1) * LANES] = scales[source, 1:2, :]
+    per = up_lines * LANES
     for q in range(n_fs // 2):
         rows = scales[y * (n_fs // 2) + q]
-        for i in range(per // 128):
-            scale_up[:, q * per + i * 128:q * per + (i + 1) * 128] = rows[3 + i:4 + i, :]
+        for i in range(up_lines):
+            scale_up[:, q * per + i * LANES:q * per + (i + 1) * LANES] = rows[2 + i:3 + i, :]
 
     for source_z in range(n_z):
         for kind in range(2):
@@ -553,7 +562,7 @@
         total = (mixed[rows, :].astype(f32) + product * scale_out[...]).astype(bf16)
         mixed[rows, :] = total
         floats = total.astype(f32)
-        squares[0, rows, :] = jnp.broadcast_to(jnp.sum(floats * floats, axis=1, keepdims=True), (tile, 128))
+        squares[0, rows, :] = jnp.broadcast_to(jnp.sum(floats * floats, axis=1, keepdims=True), (tile, LANES))
         return carry
 
     lax.fori_loop(0, n_tiles, mix_rows, 0)
@@ -568,7 +577,7 @@
         total = squares[0, rows, :] + squares[1, rows, :]
         scale = lax.rsqrt(total[:, :1] * (1.0 / width) + epsilon)
         floats = mixed[rows, :].astype(f32)
-        ffn_rows[0, rows, my_half] = (floats * scale * ffn_gain[pl.ds(tp, 1), :]).astype(bf16)
+        ffn_rows[0, rows, my_half] = (floats * scale * ffn_gain[:, my_half]).astype(bf16)
         act_pair_copy(t).start()
         act_core_copy(0, t).start()
         return carry
@@ -622,16 +631,17 @@
     outer_pass(1, 6)
     lax.fori_loop(half_tiles, 2 * half_tiles, up_tiles(1), 0)
 
-    down_rows = DOWN_ROWS
-
-    def part_core_copy(index, sequence):
-        span = pl.ds(sequence * length, length)
+    down_rows, n_parts = DOWN_ROWS, length // DOWN_ROWS
+
+    def part_core_copy(index, sequence, m):
+        span = pl.ds(pl.multiple_of(sequence * length + m * down_rows, down_rows), down_rows)
         return remote(core_sent.at[index, span, :], core_got.at[index, span, :],
-                      part_core_send.at[index, sequence], part_core_recv.at[index, sequence], core)
-
-    def part_pair_copy(index):
-        return remote(pair_sent.at[index], pair_got.at[index],
-                      part_pair_send.at[index], part_pair_recv.at[index], pair)
+                      part_core_send.at[index, sequence, m], part_core_recv.at[index, sequence, m], core)
+
+    def part_pair_copy(index, m):
+        span = pl.ds(pl.multiple_of(m * down_rows, down_rows), down_rows)
+        return remote(pair_sent.at[index, span, :], pair_got.at[index, span, :],
+                      part_pair_send.at[index, m], part_pair_recv.at[index, m], pair)
 
     def down_order(n):
         return jnp.where(n < n_z, 2 * n, 2 * (n - n_z) + 1)
@@ -657,45 +667,53 @@
 
         index = source % owned
         mine = source // owned == tp
-        scale = jnp.concatenate([scales[source, 7:8, :], scales[source, 8:9, :]], axis=1)
-        for sequence in (1, 0):
-            def down_tile_rows(m, inner):
-                rows = pl.ds(pl.multiple_of(m * down_rows, down_rows), down_rows)
-                product = jnp.dot(hidden[sequence, rows, :], down_all[source], preferred_element_type=f32) * scale
-
-                @pl.when(mine)
-                def _():
-                    if sequence == 1:
-                        pair_total[rows, :] = product
-                    else:
-                        totals[index, rows, :] = product
-
-                @pl.when(jnp.logical_not(mine))
-                def _():
-                    there = pl.ds(pl.multiple_of(sequence * length + m * down_rows, down_rows), down_rows)
-                    core_sent[index, there, :] = product.astype(bf16)
-
-                return inner
-
-            lax.fori_loop(0, length // down_rows, down_tile_rows, 0)
+        lines = [2 + up_lines + i for i in range(down_lines)]
+        scale = jnp.concatenate([scales[source, line:line + 1, :] for line in lines], axis=1)
+
+        def part(sequence, m):
+            rows = pl.ds(pl.multiple_of(m * down_rows, down_rows), down_rows)
+            product = jnp.dot(hidden[sequence, rows, :], down_all[source], preferred_element_type=f32) * scale
+
+            @pl.when(mine)
+            def _():
+                if sequence == 1:
+                    pair_total[rows, :] = product
+                else:
+                    totals[index, rows, :] = product
 
             @pl.when(jnp.logical_not(mine))
             def _():
-                part_core_copy(index, sequence).start()
-
-        @pl.when(mine)
-        def _():
-            part_core_copy(index, 1).wait_recv()
-            pair_sent[index] = (pair_total[...] + core_got[index, length:2 * length, :].astype(f32)).astype(bf16)
-            part_pair_copy(index).start()
-
+                core_sent[index, pl.ds(pl.multiple_of(sequence * length + m * down_rows, down_rows), down_rows), :] = product.astype(bf16)
+                part_core_copy(index, sequence, m).start()
+
+        def hand_over(m):
+            @pl.when(mine)
+            def _():
+                rows = pl.ds(pl.multiple_of(m * down_rows, down_rows), down_rows)
+                part_core_copy(index, 1, m).wait_recv()
+                got = core_got[index, pl.ds(pl.multiple_of(length + m * down_rows, down_rows), down_rows), :].astype(f32)
+                pair_sent[index, rows, :] = (pair_total[rows, :] + got).astype(bf16)
+                part_pair_copy(index, m).start()
+
+        def theirs(m, inner_carry):
+            part(1, m)
+            return inner_carry
+
+        def ours(m, inner_carry):
+            hand_over(m)
+            part(0, m)
+            return inner_carry
+
+        lax.fori_loop(0, n_parts, theirs, 0)
+        lax.fori_loop(0, n_parts, ours, 0)
         return carry
 
     lax.fori_loop(0, n_fs, down_block, 0)
 
-    def store_block(index):
+    def store_block(index, m):
+        rows = pl.ds(pl.multiple_of(m * down_rows, down_rows), down_rows)
         columns = pl.ds(pl.multiple_of(index * block, block), block)
-        return pltpu.make_async_copy(pair_sent.at[index], out.at[:, columns], store_sem.at[index])
+        return pltpu.make_async_copy(pair_sent.at[index, rows, :], out.at[rows, columns], store_sem.at[index, m])
 
     def finish_block(i, carry):
         source, _ = at_step(down_order(i))
@@ -704,11 +722,14 @@
         def _():
             index = source % owned
             columns = pl.ds(pl.multiple_of(index * block, block), block)
-            part_core_copy(index, 0).wait_recv()
-            part_pair_copy(index).wait()
-            total = totals[index] + core_got[index, 0:length, :].astype(f32) + pair_got[index].astype(f32)
-            pair_sent[index] = (mixed[:, columns].astype(f32) + total).astype(bf16)
-            store_block(index).start()
+            for m in range(n_parts):
+                rows = pl.ds(pl.multiple_of(m * down_rows, down_rows), down_rows)
+                part_core_copy(index, 0, m).wait_recv()
+                part_pair_copy(index, m).wait()
+                total = totals[index, rows, :] + core_got[index, rows, :].astype(f32)
+                total = total + pair_got[index, rows, :].astype(f32)
+                pair_sent[index, rows, :] = (mixed[rows, columns].astype(f32) + total).astype(bf16)
+                store_block(index, m).start()
 
         return carry
 
@@ -755,14 +776,14 @@
         for which in range(2):
             act_core_copy(which, t).wait_send()
     for index in range(owned):
-        for sequence in range(2):
-            part_core_copy(index, sequence).wait_send()
-        store_block(index).wait()
+        for m in range(n_parts):
+            for sequence in range(2):
+                part_core_copy(index, sequence, m).wait_send()
+            store_block(index, m).wait()
 
 
 def fused(n_fs, n_tp, stream, norm_gain, w_in, s_in, pool_w, w_out, s_out,
           ffn_gain, w_up, s_up, w_down, s_down):
-    fs = lax.axis_index("fs")
     tokens = stream[0]
     length, local = tokens.shape
     rows, all_units = w_up.shape
@@ -771,15 +792,14 @@
     in_rows, pool_width = w_in.shape
     out_rows = w_out.shape[0]
     owned = n_fs // n_tp
-    placed_in = lax.dynamic_update_slice(jnp.zeros((pool_width,), f32), s_in, (fs * s_in.shape[0],))
-    packed = jnp.concatenate([placed_in, s_out, s_up, s_down])
-    packed = jnp.pad(packed, (0, 16 * 128 - packed.shape[0])).reshape(16, 128)
+    parts = length // DOWN_ROWS
+    lines = -(-(2 + (s_up.shape[0] + block) // LANES) // 8) * 8
     vmem, anywhere = pl.BlockSpec(memory_space=pltpu.VMEM), pl.BlockSpec(memory_space=pl.ANY)
     dma = pltpu.SemaphoreType.DMA
     result = pl.pallas_call(
         functools.partial(fused_kernel, n_fs, n_tp),
         out_shape=jax.ShapeDtypeStruct((length, local), bf16),
-        in_specs=[anywhere] * 3 + [vmem] * 6,
+        in_specs=[anywhere] * 3 + [vmem] * 9,
         out_specs=anywhere,
         scratch_shapes=[
             pltpu.VMEM((rows * n_fs, units), bf16),
@@ -793,7 +813,7 @@
             pltpu.VMEM((out_rows * n_fs, local), bf16),
             pltpu.VMEM((length, pool_width), bf16),
             pltpu.VMEM((length, n_tp * pool_width), bf16),
-            pltpu.VMEM((2, length, 128), f32),
+            pltpu.VMEM((2, length, LANES), f32),
             pltpu.VMEM((owned, 2 * length, block), bf16),
             pltpu.VMEM((owned, 2 * length, block), bf16),
             pltpu.VMEM((owned, length, block), bf16),
@@ -801,7 +821,8 @@
             pltpu.VMEM((owned, length, block), f32),
             pltpu.VMEM((length, block), f32),
             pltpu.VMEM((rows, units), f32),
-            pltpu.VMEM((n_fs, 16, 128), f32),
+            pltpu.VMEM((lines, LANES), f32),
+            pltpu.VMEM((n_fs, lines, LANES), f32),
             pltpu.VMEM((1, pool_width), f32),
             pltpu.VMEM((1, local), f32),
             pltpu.VMEM((1, units), f32),
@@ -810,24 +831,25 @@
             dma((2, n_fs, 2, PARTS)), dma((2, 2, 2, PARTS)), dma((2, n_fs, PARTS)), dma((2, n_fs, PARTS)),
             dma((2, 2, PARTS)),
             dma((4,)), dma((4,)), dma((2, 4)), dma((2, 4)), dma((4,)), dma((4,)),
-            dma((owned, 2)), dma((owned, 2)), dma((owned,)), dma((owned,)), dma((owned,)),
+            dma((owned, 2, parts)), dma((owned, 2, parts)), dma((owned, parts)), dma((owned, parts)), dma((owned, parts)),
         ],
         compiler_params=pltpu.CompilerParams(
             collective_id=0, has_side_effects=True, vmem_limit_bytes=VMEM_BYTES
         ),
         name="fused_layer",
     )(tokens, w_up, w_down, w_in, w_out, pool_w,
-      norm_gain.reshape(n_tp, local), ffn_gain.reshape(n_tp, local), packed)
+      norm_gain[None], ffn_gain[None], s_in[None], s_out[None], s_up[None], s_down[None])
     return result[None]
 
 
 def fits(n_rep, n_fs, n_tp, args):
-    stream, w_in, pool_w, w_down = args[0], args[2], args[4], args[10]
+    stream, w_in, pool_w, s_out, s_up, w_down = args[0], args[2], args[4], args[6], args[9], args[10]
     return (
         n_rep == 2 and n_tp == 2 and n_fs % 4 == 0
         and stream.shape[0] == 1
         and pool_w.shape[0] * GROUP == w_in.shape[1] * n_tp
         and stream.shape[2] * n_tp == w_down.shape[1] * n_fs
+        and s_out.shape[0] == LANES and s_up.shape[0] % LANES == 0 and w_down.shape[1] % LANES == 0
     )
 
 

time: 191 us -> 184 us (0.963)
  local copies, waits for them, and re-layouts: 6.52 us -> 3.08 us
  Pallas kernels: 183 us -> 180 us
    reshape x2 -> x0, local copies, waits for them, and re-layouts: 2.6 us -> none  [the longest x1 1.3 us: fused(): norm_gain.reshape(n_tp, local)]
    pallas_call x1, Pallas kernels: 183 us -> 180 us  [fused(): pl.pallas_call(functools.partial(fused_kernel, n_fs, n_tp), out_shape=jax...]
where the time goes in v2:
time: 184 us; the launch traced here: 183 us
  Pallas kernels  180 us (98%)
  local copies, waits for them, and re-layouts  3.08 us (2%)
    pallas_call x1, Pallas kernels, fused(): pl.pallas_call(functools.partial(fused_kernel, n_fs, n_tp), out_shape=jax...  180 us

profile of v2, /device:TPU:1, one launch (start us, length us, event | category | flops | bytes accessed | tf_op | source)
XLA Modules:
  0.0 183.4 jit_solution(8462705218230547650)
XLA Ops:
  0.0 180.4 %fused_layer.1 = bf16[1024,1024]{1,0:T(8,128)(2,1)} custom-call(bf16[1024,1024]{1,0:T(8,128)(2,1)} %bitcast.9, f32[256,4096]{1,0:T(8,128)} %w_up.1, f32[4096,256]{1,0:T(8,128)} %w_down.1, f32[256,256]{1,0:T(8,128)} %w_in.1, f32[64,1024]{1,0:T(8,128)} %w_out.1, bf16[4,128,128]{2,1,0:T(8,128)(2,1)} %pool_w.1, f32[1,2048]{1,0:T(1,128)} %bitcast.10, ...), custom_call_target="tpu_custom_call" | custom-call | tf_op jit(solution)/shard_map/fused_layer/pallas_call | solution.py:799
  180.4 3.1 %copy.14 = bf16[1,1024,1024]{2,1,0:T(8,128)(2,1)} copy(bf16[1,1024,1024]{2,1,0:T(8,128)(2,1)} %bitcast.8) | data formatting | bytes 4194304

commit v3 on v2

--- a/solution.py
+++ b/solution.py
@@ -303,10 +303,10 @@
             piece_wait(kind, fs + 1 - 2 * y, rep, q)
             both_sides(lambda side, q=q: own_copy(kind, 1, side, q).start())
 
-    def pass_on(kind, i):
+    def pass_on(kind, i, parts=range(PARTS)):
         source, left = at_step(i)
         going, device = onward(left)
-        for q in range(PARTS):
+        for q in parts:
             piece_wait(kind, source, rep, q)
 
             @pl.when(going)
@@ -485,10 +485,10 @@
         def _():
             pass_on(kind, i)
 
-    def outer_pass(kind, i):
+    def outer_pass(kind, i, parts=range(PARTS)):
         @pl.when(jnp.logical_not(inner))
         def _():
-            pass_on(kind, i)
+            pass_on(kind, i, parts)
 
     for j in range(1, n_z):
         source, _ = at_step(2 * j)
@@ -592,6 +592,9 @@
     inner_pass(1, 2)
     inner_pass(1, 4)
     inner_pass(1, 6)
+    for t in range(n_tiles):
+        act_pair_copy(t).wait_recv()
+        act_core_copy(1, t).start()
     other_half(0, fs + 1 - 2 * y)
 
     def up_ready(i, carry):
@@ -618,19 +621,6 @@
 
         return body
 
-    for t in range(n_tiles):
-        act_pair_copy(t).wait_recv()
-        act_core_copy(1, t).start()
-    lax.fori_loop(0, half_tiles, up_tiles(0), 0)
-    outer_pass(1, 4)
-    lax.fori_loop(half_tiles, 2 * half_tiles, up_tiles(0), 0)
-    pass_pair(1)
-    for t in range(n_tiles):
-        act_core_copy(1, t).wait_recv()
-    lax.fori_loop(0, half_tiles, up_tiles(1), 0)
-    outer_pass(1, 6)
-    lax.fori_loop(half_tiles, 2 * half_tiles, up_tiles(1), 0)
-
     down_rows, n_parts = DOWN_ROWS, length // DOWN_ROWS
 
     def part_core_copy(index, sequence, m):
@@ -646,65 +636,157 @@
     def down_order(n):
         return jnp.where(n < n_z, 2 * n, 2 * (n - n_z) + 1)
 
+    def block_of(n):
+        source, _ = at_step(down_order(n))
+        return source, source % owned, source // owned == tp
+
+    def part(n, sequence, m):
+        source, index, mine = block_of(n)
+        lines = [2 + up_lines + i for i in range(down_lines)]
+        scale = jnp.concatenate([scales[source, line:line + 1, :] for line in lines], axis=1)
+        rows = pl.ds(pl.multiple_of(m * down_rows, down_rows), down_rows)
+        product = jnp.dot(hidden[sequence, rows, :], down_all[source], preferred_element_type=f32) * scale
+
+        @pl.when(mine)
+        def _():
+            if sequence == 1:
+                pair_total[rows, :] = product
+            else:
+                totals[index, rows, :] = product
+
+        @pl.when(jnp.logical_not(mine))
+        def _():
+            start = pl.multiple_of(sequence * length + m * down_rows, down_rows)
+            core_sent[index, pl.ds(start, down_rows), :] = product.astype(bf16)
+            part_core_copy(index, sequence, m).start()
+
+    def hand_part(n, m):
+        _, index, mine = block_of(n)
+
+        @pl.when(mine)
+        def _():
+            rows = pl.ds(pl.multiple_of(m * down_rows, down_rows), down_rows)
+            part_core_copy(index, 1, m).wait_recv()
+            got = core_got[index, pl.ds(pl.multiple_of(length + m * down_rows, down_rows), down_rows), :].astype(f32)
+            pair_sent[index, rows, :] = (pair_total[rows, :] + got).astype(bf16)
+            part_pair_copy(index, m).start()
+
+    def theirs(n):
+        def body(m, carry):
+            part(n, 1, m)
+            return carry
+
+        lax.fori_loop(0, n_parts, body, 0)
+
+    def hand_over(n):
+        def body(m, carry):
+            hand_part(n, m)
+            return carry
+
+        lax.fori_loop(0, n_parts, body, 0)
+
+    outer_pass(1, 4, range(1))
+    for t in range(n_tiles):
+        act_core_copy(1, t).wait_recv()
+    lax.fori_loop(0, 3, up_tiles(1), 0)
+    outer_pass(1, 4, range(1, PARTS))
+    lax.fori_loop(3, 2 * half_tiles, up_tiles(1), 0)
+    outer_pass(1, 6, range(1))
+    theirs(0)
+    pass_pair(1)
+    lax.fori_loop(0, half_tiles, up_tiles(0), 0)
+    hand_over(0)
+    other_half(1, at_step(down_order(1))[0])
+    theirs(1)
+    outer_pass(1, 6, range(1, PARTS))
+    lax.fori_loop(half_tiles, 2 * half_tiles, up_tiles(0), 0)
+    hand_over(1)
+
+    def sent_first():
+        for kind in range(2):
+            both_sides(lambda side, kind=kind: mix_own_copy(kind, side).wait_send())
+            for q in range(PARTS):
+                for order in range(2):
+                    both_sides(lambda side, kind=kind, order=order, q=q: own_copy(kind, order, side, q).wait_send())
+                for half in range(2):
+                    pair_copy(kind, half, q).wait_send()
+            for half in range(2):
+                mix_pair_copy(kind, fs, half).wait_send()
+
+        def sent_step(i, carry):
+            source, left = at_step(i)
+            going, device = onward(left)
+            for q in range(PARTS):
+                @pl.when(going)
+                def _():
+                    onward_copy(0, source, q, device).wait_send()
+
+                across_copy(0, source, q).wait_send()
+
+            @pl.when(i % 2 == 0)
+            def _():
+                for kind in range(2):
+                    @pl.when(going)
+                    def _():
+                        mix_onward_copy(kind, source, device).wait_send()
+
+                    mix_across_copy(kind, source).wait_send()
+                    mix_pair_copy(kind, source, 0).wait_send()
+                    mix_pair_copy(kind, source, 1).wait_send()
+
+            return carry
+
+        lax.fori_loop(2, 2 * n_z, sent_step, 0)
+        for offset in range(1, n_fs):
+            scale_copy(offset).wait_send()
+        for t in range(n_tiles):
+            act_pair_copy(t).wait_send()
+            for which in range(2):
+                act_core_copy(which, t).wait_send()
+
     def down_block(n, carry):
         @pl.when(inner & (n >= 1) & (n < n_z - 1))
         def _():
             pass_on(1, 2 * n + 1)
 
-        @pl.when(jnp.logical_not(inner) & (n % 2 == 1) & (n < 2 * n_z - 4))
-        def _():
-            pass_on(1, n + 2)
-
-        @pl.when(n == 2 * n_z - 3)
+        @pl.when(jnp.logical_not(inner) & (n % 2 == 1) & (n >= 3) & (n < 2 * n_z - 2))
+        def _():
+            pass_on(1, n + 2, range(1, PARTS))
+
+        @pl.when(inner & (n == 2 * n_z - 3))
         def _():
             pass_on(1, 2 * n_z - 1)
 
         source, _ = at_step(down_order(n))
 
-        @pl.when(n > 0)
+        @pl.when(n == 2 * n_z - 1)
+        def _():
+            sent_first()
+
+        @pl.when(n > 1)
         def _():
             other_half(1, source)
 
-        index = source % owned
-        mine = source // owned == tp
-        lines = [2 + up_lines + i for i in range(down_lines)]
-        scale = jnp.concatenate([scales[source, line:line + 1, :] for line in lines], axis=1)
-
-        def part(sequence, m):
-            rows = pl.ds(pl.multiple_of(m * down_rows, down_rows), down_rows)
-            product = jnp.dot(hidden[sequence, rows, :], down_all[source], preferred_element_type=f32) * scale
-
-            @pl.when(mine)
+        @pl.when(n > 1)
+        def _():
+            theirs(n)
+
+        @pl.when(jnp.logical_not(inner) & (n % 2 == 0) & (n < 2 * n_z - 3))
+        def _():
+            pass_on(1, n + 3, range(1))
+
+        @pl.when(jnp.logical_not(inner) & (n == 1))
+        def _():
+            pass_on(1, 3, range(1, PARTS))
+
+        def ours(m, inner_carry):
+            @pl.when(n > 1)
             def _():
-                if sequence == 1:
-                    pair_total[rows, :] = product
-                else:
-                    totals[index, rows, :] = product
-
-            @pl.when(jnp.logical_not(mine))
-            def _():
-                core_sent[index, pl.ds(pl.multiple_of(sequence * length + m * down_rows, down_rows), down_rows), :] = product.astype(bf16)
-                part_core_copy(index, sequence, m).start()
-
-        def hand_over(m):
-            @pl.when(mine)
-            def _():
-                rows = pl.ds(pl.multiple_of(m * down_rows, down_rows), down_rows)
-                part_core_copy(index, 1, m).wait_recv()
-                got = core_got[index, pl.ds(pl.multiple_of(length + m * down_rows, down_rows), down_rows), :].astype(f32)
-                pair_sent[index, rows, :] = (pair_total[rows, :] + got).astype(bf16)
-                part_pair_copy(index, m).start()
-
-        def theirs(m, inner_carry):
-            part(1, m)
+                hand_part(n, m)
+
+            part(n, 0, m)
             return inner_carry
 
-        def ours(m, inner_carry):
-            hand_over(m)
-            part(0, m)
-            return inner_carry
-
-        lax.fori_loop(0, n_parts, theirs, 0)
         lax.fori_loop(0, n_parts, ours, 0)
         return carry
 
@@ -735,46 +817,19 @@
 
     lax.fori_loop(0, n_fs, finish_block, 0)
 
-    for kind in range(2):
-        both_sides(lambda side, kind=kind: mix_own_copy(kind, side).wait_send())
+    def sent_last(i, carry):
+        source, left = at_step(i)
+        going, device = onward(left)
         for q in range(PARTS):
-            for order in range(2):
-                both_sides(lambda side, kind=kind, order=order, q=q: own_copy(kind, order, side, q).wait_send())
-            for half in range(2):
-                pair_copy(kind, half, q).wait_send()
-        for half in range(2):
-            mix_pair_copy(kind, fs, half).wait_send()
-
-        def sent_step(i, carry, kind=kind):
-            source, left = at_step(i)
-            going, device = onward(left)
-
-            for q in range(PARTS):
-                @pl.when(going)
-                def _():
-                    onward_copy(kind, source, q, device).wait_send()
-
-                across_copy(kind, source, q).wait_send()
-
-            @pl.when(i % 2 == 0)
+            @pl.when(going)
             def _():
-                @pl.when(going)
-                def _():
-                    mix_onward_copy(kind, source, device).wait_send()
-
-                mix_across_copy(kind, source).wait_send()
-                mix_pair_copy(kind, source, 0).wait_send()
-                mix_pair_copy(kind, source, 1).wait_send()
-
-            return carry
-
-        lax.fori_loop(2, 2 * n_z, sent_step, 0)
-    for offset in range(1, n_fs):
-        scale_copy(offset).wait_send()
-    for t in range(n_tiles):
-        act_pair_copy(t).wait_send()
-        for which in range(2):
-            act_core_copy(which, t).wait_send()
+                onward_copy(1, source, q, device).wait_send()
+
+            across_copy(1, source, q).wait_send()
+
+        return carry
+
+    lax.fori_loop(2, 2 * n_z, sent_last, 0)
     for index in range(owned):
         for m in range(n_parts):
             for sequence in range(2):

time: 184 us -> 182 us (0.989)
  Pallas kernels: 180 us -> 178 us
    pallas_call x1, Pallas kernels: 180 us -> 178 us  [fused(): pl.pallas_call(functools.partial(fused_kernel, n_fs, n_tp), out_shape=jax...]
where the time goes in v3:
time: 182 us; the launch traced here: 181 us
  Pallas kernels  178 us (98%)
  local copies, waits for them, and re-layouts  3.08 us (2%)
    pallas_call x1, Pallas kernels, fused(): pl.pallas_call(functools.partial(fused_kernel, n_fs, n_tp), out_shape=jax...  178 us

profile of v3, /device:TPU:1, one launch (start us, length us, event | category | flops | bytes accessed | tf_op | source)
XLA Modules:
  0.0 181.5 jit_solution(16720054235985472190)
XLA Ops:
  0.0 178.4 %fused_layer.1 = bf16[1024,1024]{1,0:T(8,128)(2,1)} custom-call(bf16[1024,1024]{1,0:T(8,128)(2,1)} %bitcast.9, f32[256,4096]{1,0:T(8,128)} %w_up.1, f32[4096,256]{1,0:T(8,128)} %w_down.1, f32[256,256]{1,0:T(8,128)} %w_in.1, f32[64,1024]{1,0:T(8,128)} %w_out.1, bf16[4,128,128]{2,1,0:T(8,128)(2,1)} %pool_w.1, f32[1,2048]{1,0:T(1,128)} %bitcast.10, ...), custom_call_target="tpu_custom_call" | custom-call | tf_op jit(solution)/shard_map/fused_layer/pallas_call | solution.py:854
  178.4 3.1 %copy.14 = bf16[1,1024,1024]{2,1,0:T(8,128)(2,1)} copy(bf16[1,1024,1024]{2,1,0:T(8,128)(2,1)} %bitcast.8) | data formatting | bytes 4194304
